TPU v7x, 32 devices: a whole 2x2x4 slice. The times are simulated.
32 devices in a mesh: fs: 8 (over z, x), tp: 4 (over y, core).
Axes of the slice: x: 2, y: 2, z: 4, core: 2. Of those that a mesh axis runs over, the one named last changes fastest.
Arguments:
- later_input: bfloat16 [4096, 2048], P(('fs', 'tp')), may hold values from -6 to 6
- saved_input: bfloat16 [4096, 2048], P(('fs', 'tp')), may hold values from -6 to 6
- cotangent: bfloat16 [4096, 3072], P('fs', 'tp'), may hold values from -6 to 6
- up_weight: bfloat16 [2048, 3072], P('fs', 'tp'), may hold values from -0.125 to 0.125
- gate_weight: bfloat16 [2048, 3072], P('fs', 'tp'), may hold values from -0.125 to 0.125
- up_taps: bfloat16 [3, 3072], replicated, may hold values from -3.5 to 3.5
- gate_taps: bfloat16 [3, 3072], replicated, may hold values from -3.5 to 3.5
- up_grad_sum: float32 [2048, 3072], P('fs', 'tp'), may hold values from -6 to 6
- gate_grad_sum: float32 [2048, 3072], P('fs', 'tp'), may hold values from -6 to 6
- up_taps_sum: float32 [3, 3072], replicated, may hold values from -6 to 6
- gate_taps_sum: float32 [3, 3072], replicated, may hold values from -6 to 6
Outputs:
- hidden: bfloat16 [4096, 3072], P('fs', 'tp')
- input_grad: bfloat16 [4096, 2048], P(('fs', 'tp'))
- new_up_sum: float32 [2048, 3072], P('fs', 'tp')
- new_gate_sum: float32 [2048, 3072], P('fs', 'tp')
- new_up_taps_sum: float32 [3, 3072], replicated
- new_gate_taps_sum: float32 [3, 3072], replicated
All inputs are finite; a program needn't handle non-finite values.
Results may differ from a plain program's by a relative error of at most 0.018.
Values may be sent and summed in bfloat16 or wider, within the bound.
A program may use at most 64 MiB of HBM per device.

v0:
```python
import jax
import jax.numpy as jnp
from jax import lax
from jax.sharding import PartitionSpec as P


def delayed(values, steps):
    zeros = jnp.zeros_like(values[:steps])
    return jnp.concatenate([zeros, values[:-steps]], axis=0)


def advanced(values, steps):
    zeros = jnp.zeros_like(values[:steps])
    return jnp.concatenate([values[steps:], zeros], axis=0)


def depthwise(values, taps):
    return taps[2] * values + taps[1] * delayed(values, 1) + taps[0] * delayed(values, 2)


def depthwise_back(grads, taps):
    return taps[2] * grads + taps[1] * advanced(grads, 1) + taps[0] * advanced(grads, 2)


def taps_grad(grads, values):
    return jnp.stack(
        [
            jnp.sum(grads * delayed(values, 2), axis=0),
            jnp.sum(grads * delayed(values, 1), axis=0),
            jnp.sum(grads * values, axis=0),
        ],
        axis=0,
    )


def make_term(rows_all, grads):
    return lax.dot_general(
        rows_all, grads, (((0,), (0,)), ((), ())), preferred_element_type=jnp.float32
    )


def shards(
    later_input,
    saved_input,
    cotangent,
    up_weight,
    gate_weight,
    up_taps,
    gate_taps,
    up_grad_sum,
    gate_grad_sum,
    up_taps_sum,
    gate_taps_sum,
):
    column_count = up_weight.shape[1]
    group_size = lax.axis_size("tp")
    offset = lax.axis_index("tp") * column_count
    tokens_all = later_input.shape[0] * lax.axis_size("fs") * group_size
    grad_scale = jnp.float32(tokens_all ** (-0.5))
    taps_both = jnp.concatenate(
        [
            lax.dynamic_slice_in_dim(up_taps, offset, column_count, 1),
            lax.dynamic_slice_in_dim(gate_taps, offset, column_count, 1),
        ],
        axis=1,
    ).astype(jnp.float32)
    weight_both = jnp.concatenate([up_weight, gate_weight], axis=1)
    later_rows = lax.all_gather(later_input, "tp", axis=0, tiled=True)
    saved_rows = lax.all_gather(saved_input, "tp", axis=0, tiled=True)
    shard_rows = lax.all_gather(weight_both, "fs", axis=0, tiled=True)
    proj_later = jnp.dot(later_rows, shard_rows, preferred_element_type=jnp.float32)
    proj_saved = jnp.dot(saved_rows, shard_rows, preferred_element_type=jnp.float32)
    conv_later = depthwise(proj_later.astype(jnp.bfloat16).astype(jnp.float32), taps_both)
    hidden = (jax.nn.silu(conv_later[:, column_count:]) * conv_later[:, :column_count]).astype(
        jnp.bfloat16
    )
    saved_proj = proj_saved.astype(jnp.bfloat16)
    saved_proj32 = saved_proj.astype(jnp.float32)
    conv_saved = depthwise(saved_proj32, taps_both)
    saved_up = conv_saved[:, :column_count]
    saved_gate = conv_saved[:, column_count:]
    sigmoid_gate = jax.nn.sigmoid(saved_gate)
    upstream = cotangent.astype(jnp.float32)
    grad_conv = jnp.concatenate(
        [
            upstream * jax.nn.silu(saved_gate),
            upstream * saved_up * sigmoid_gate * (1.0 + saved_gate * (1.0 - sigmoid_gate)),
        ],
        axis=1,
    )
    grad_proj = depthwise_back(grad_conv, taps_both).astype(jnp.bfloat16)
    taps_local = taps_grad(grad_conv, saved_proj32)
    total_cols = column_count * group_size
    taps_up_full = lax.dynamic_update_slice_in_dim(
        jnp.zeros((3, total_cols), jnp.float32), taps_local[:, :column_count], offset, 1
    )
    taps_gate_full = lax.dynamic_update_slice_in_dim(
        jnp.zeros((3, total_cols), jnp.float32), taps_local[:, column_count:], offset, 1
    )
    taps_up_total, taps_gate_total = lax.psum((taps_up_full, taps_gate_full), ("fs", "tp"))
    weight_grad = lax.psum_scatter(
        make_term(saved_rows, grad_proj).astype(jnp.bfloat16), "fs", scatter_dimension=0, tiled=True
    ).astype(jnp.float32)
    up_grad = weight_grad[:, :column_count]
    gate_grad = weight_grad[:, column_count:]
    partial_grad = lax.dot_general(
        grad_proj,
        lax.all_gather(weight_both, "fs", axis=0, tiled=True),
        (((1,), (1,)), ((), ())),
        preferred_element_type=jnp.float32,
    )
    input_grad = lax.psum_scatter(
        partial_grad.astype(jnp.bfloat16), "tp", scatter_dimension=0, tiled=True
    )
    new_up_sum = up_grad_sum + grad_scale * up_grad
    new_gate_sum = gate_grad_sum + grad_scale * gate_grad
    new_up_taps_sum = up_taps_sum + grad_scale * taps_up_total
    new_gate_taps_sum = gate_taps_sum + grad_scale * taps_gate_total
    return (hidden, input_grad, new_up_sum, new_gate_sum, new_up_taps_sum, new_gate_taps_sum)


def solution(mesh):
    return jax.shard_map(
        shards,
        mesh=mesh,
        in_specs=(
            P(("fs", "tp"), None),
            P(("fs", "tp"), None),
            P("fs", "tp"),
            P("fs", "tp"),
            P("fs", "tp"),
            P(),
            P(),
            P("fs", "tp"),
            P("fs", "tp"),
            P(),
            P(),
        ),
        out_specs=(P("fs", "tp"), P(("fs", "tp"), None), P("fs", "tp"), P("fs", "tp"), P(), P()),
        check_vma=False,
    )
```

profile of v0, /device:TPU:24, one launch (start us, length us, event | category | flops | bytes accessed | tf_op | source)
XLA Modules:
  0.0 458.0 jit_solution(4171032246797810518)
XLA Ops:
  8.0 2.0 pad_maximum_fusion.1
  10.8 1.2 copy.17
  12.8 20.4 %all-gather.8.cloned.1.call-done = bf16[512,2048]{1,0:T(8,128)(2,1)} async-done(((bf16[128,2048]{1,0:T(8,128)(2,1)}), bf16[512,2048]{1,0:T(8,128)(2,1)}) %all-gather.8.cloned.1.call-update) | async-done | bytes 2097168 | tf_op jit(solution)/shard_map/all_gather | solution.py:69
  33.1 99.6 %all-gather.4.cloned.1.call-done = bf16[2048,1536]{1,0:T(8,128)(2,1)} async-done(((bf16[256,1536]{1,0:T(8,128)(2,1)}), bf16[2048,1536]{1,0:T(8,128)(2,1)}) %all-gather.4.cloned.1.call-update) | async-done | bytes 6291472 | tf_op jit(solution)/shard_map/all_gather | solution.py:70
  132.7 6.2 %convert_bitcast_fusion = f32[512,1536]{0,1:T(8,128)S(1)} fusion(bf16[2048,1536]{1,0:T(8,128)(2,1)} %all-gather.4.cloned.1.call-done, bf16[512,2048]{1,0:T(8,128)(2,1)} %all-gather.8.cloned.1.call-done), kind=kOutput, calls=%fused_computation.9 | convolution fusion | flops 3222798336 | bytes 11534336 | tf_op jit(solution)/shard_map/dot_general | solution.py:72
  139.0 2.6 multiply_add_fusion
  142.6 2.7 fusion.1
  145.3 2.6 fusion.2
  147.9 9.0 %all-gather.6.cloned.1.call-done = bf16[512,2048]{1,0:T(8,128)(2,1)} async-done(((bf16[128,2048]{1,0:T(8,128)(2,1)}), bf16[512,2048]{1,0:T(8,128)(2,1)}) %all-gather.6.cloned.1.call-update) | async-done | bytes 2097168 | tf_op jit(solution)/shard_map/all_gather | solution.py:68
  156.9 6.4 %convert_bitcast_fusion.1 = f32[512,1536]{0,1:T(8,128)S(1)} fusion(bf16[2048,1536]{1,0:T(8,128)(2,1)} %all-gather.4.cloned.1.call-done, bf16[512,2048]{1,0:T(8,128)(2,1)} %all-gather.6.cloned.1.call-done), kind=kOutput, calls=%fused_computation.10 | convolution fusion | flops 3222798336 | bytes 11534336 | tf_op jit(solution)/shard_map/dot_general | solution.py:71
  163.4 7.4 %multiply_reduce_fusion.2 = (f32[1536]{0:T(1024)S(1)}, f32[1536]{0:T(1024)S(1)}, f32[1536]{0:T(1024)S(1)}, bf16[512,1536]{0,1:T(8,128)(2,1)}, f32[512,1536]{0,1:T(8,128)}) fusion(f32[510,1536]{0,1:T(8,128)S(1)} %bitcast.20, f32[512,768]{0,1:T(8,128)S(1)} %copy-done.1, f32[512,768]{0,1:T(8,128)S(1)} %copy-done.3, f32[512,1536]{0,1:T(8,128)S(1)} %convert_bitcast_fusion, ...), kind=kLoop, calls=%fused_computation.13 | loop fusion | flops 14151168 | bytes 33011712 | tf_op jit(solution)/shard_map/reduce_sum | solution.py:28
  171.8 8.2 %fusion = bf16[2048,1536]{0,1:T(8,128)(2,1)} fusion(bf16[512,1536]{0,1:T(8,128)(2,1)} %get-tuple-element.22, bf16[512,2048]{1,0:T(8,128)(2,1)} %all-gather.8.cloned.1.call-done), kind=kOutput, calls=%fused_computation.1 | convolution fusion | flops 3224371200 | bytes 9961472 | tf_op jit(solution)/shard_map/dot_general | solution.py:37
  180.1 1.3 copy-done.10
  181.5 7.5 %convolution_convert_fusion.1 = bf16[512,2048]{1,0:T(8,128)(2,1)} fusion(bf16[512,1536]{0,1:T(8,128)(2,1)S(1)} %copy-done.10, bf16[2048,1536]{1,0:T(8,128)(2,1)} %all-gather.4.cloned.1.call-done), kind=kOutput, calls=%fused_computation.17 | convolution fusion | flops 3222274048 | bytes 9961472 | tf_op jit(solution)/shard_map/dot_general | solution.py:106
  189.0 2.5 copy.19
  191.5 2.3 copy.20
  193.8 1.4 fusion.5
  195.1 2.4 copy.21
  197.6 98.2 %all-reduce.9.cloned.1.call-done = (f32[3,3072]{1,0:T(4,128)}, f32[3,3072]{1,0:T(4,128)}) async-done(((f32[3,3072]{1,0:T(4,128)}, f32[3,3072]{1,0:T(4,128)}), (f32[3,3072]{1,0:T(4,128)}, f32[3,3072]{1,0:T(4,128)})) %all-reduce.9.cloned.1.call-update) | async-done | bytes 73744 | tf_op jit(solution)/shard_map/psum | solution.py:100
  295.7 1.4 multiply_add_fusion.2
  297.2 1.4 multiply_add_fusion.3
  298.6 117.4 %reduce-scatter.5.cloned.1.call-done = bf16[256,1536]{0,1:T(8,128)(2,1)} async-done(((bf16[2048,1536]{0,1:T(8,128)(2,1)}), bf16[256,1536]{0,1:T(8,128)(2,1)}) %reduce-scatter.5.cloned.1.call-update) | async-done | bytes 786448 | tf_op jit(solution)/shard_map/reduce_scatter | solution.py:101
  416.1 1.2 convert_element_type.57
  419.9 31.3 %reduce-scatter.3.cloned.1.call-done = bf16[128,2048]{1,0:T(8,128)(2,1)} async-done(((bf16[512,2048]{1,0:T(8,128)(2,1)}), bf16[128,2048]{1,0:T(8,128)(2,1)}) %reduce-scatter.3.cloned.1.call-update) | async-done | bytes 524304 | tf_op jit(solution)/shard_map/reduce_scatter | solution.py:112
  (57 shorter events, 6.8 us)
Async XLA Ops:
  7.2 3.7 copy-start.11
  7.2 25.9 %all-gather.8.cloned.1.call-start = ((), (), s32[]{:S(2)}) async-start(), calls=%async_computation.4 | async-start | bytes 2621440 | tf_op jit(solution)/shard_map/all_gather | solution.py:69
  7.9 124.8 %all-gather.4.cloned.1.call-start = ((), (), s32[]{:S(2)}) async-start(), calls=%async_computation.2 | async-start | bytes 7077888 | tf_op jit(solution)/shard_map/all_gather | solution.py:70
  10.0 146.9 %all-gather.6.cloned.1.call-start = ((), (), s32[]{:S(2)}) async-start(), calls=%async_computation.3 | async-start | bytes 2621440 | tf_op jit(solution)/shard_map/all_gather | solution.py:68
  10.8 285.0 %all-reduce.9.cloned.1.call-start = ((), (), s32[]{:S(2)}) async-start(), calls=%async_computation.7 | async-start | bytes 196608 | tf_op jit(solution)/shard_map/psum | solution.py:100
  139.0 2.7 copy-start.9
  142.6 2.7 copy-start
  142.6 2.7 copy-start.2
  156.9 6.4 %copy-start.1 = (f32[512,768]{0,1:T(8,128)S(1)}, f32[512,768]{0,1:T(8,128)}, u32[]{:S(2)}) copy-start(f32[512,768]{0,1:T(8,128)} %copy-done) | copy-start | bytes 4718596
  156.9 6.4 %copy-start.3 = (f32[512,768]{0,1:T(8,128)S(1)}, f32[512,768]{0,1:T(8,128)}, u32[]{:S(2)}) copy-start(f32[512,768]{0,1:T(8,128)} %copy-done.2) | copy-start | bytes 4718596
  156.9 6.4 %copy-start.4 = (f32[511,1536]{0,1:T(8,128)S(1)}, f32[511,1536]{0,1:T(8,128)}, u32[]{:S(2)}) copy-start(f32[511,1536]{0,1:T(8,128)} %fusion.1) | copy-start | bytes 9418756
  156.9 6.4 %copy-start.5 = (f32[510,1536]{0,1:T(8,128)S(1)}, f32[510,1536]{0,1:T(8,128)}, u32[]{:S(2)}) copy-start(f32[510,1536]{0,1:T(8,128)} %fusion.2) | copy-start | bytes 9400324
  170.9 0.6 copy-start.13
  171.0 0.6 copy-start.12
  171.6 244.5 %reduce-scatter.5.cloned.1.call-start = ((), (), s32[]{:S(2)}) async-start(), calls=%async_computation.6 | async-start | bytes 7077888 | tf_op jit(solution)/shard_map/reduce_scatter | solution.py:101
  180.0 1.4 copy-start.10
  180.1 271.1 %reduce-scatter.3.cloned.1.call-start = ((), (), s32[]{:S(2)}) async-start(), calls=%async_computation.5 | async-start | bytes 2621440 | tf_op jit(solution)/shard_map/reduce_scatter | solution.py:112
  189.0 4.8 %copy-start.6 = (f32[512,1536]{0,1:T(8,128)S(1)}, f32[512,1536]{0,1:T(8,128)}, u32[]{:S(2)}) copy-start(f32[512,1536]{0,1:T(8,128)} %get-tuple-element.25) | copy-start | bytes 9437188
  193.8 102.0 %copy-start.14 = (f32[3,3072]{1,0:T(4,128)S(1)}, f32[3,3072]{1,0:T(4,128)}, u32[]{:S(2)}) copy-start(f32[3,3072]{1,0:T(4,128)} %param.21) | copy-start | bytes 110596
  193.8 103.4 %copy-start.15 = (f32[3,3072]{1,0:T(4,128)S(1)}, f32[3,3072]{1,0:T(4,128)}, u32[]{:S(2)}) copy-start(f32[3,3072]{1,0:T(4,128)} %param.20) | copy-start | bytes 110596
  195.1 222.2 %copy-start.7 = (f32[256,768]{0,1:T(8,128)S(1)}, f32[256,768]{0,1:T(8,128)}, u32[]{:S(2)}) copy-start(f32[256,768]{0,1:T(8,128)} %copy.19) | copy-start | bytes 2359300
  195.1 222.2 %copy-start.8 = (f32[256,768]{0,1:T(8,128)S(1)}, f32[256,768]{0,1:T(8,128)}, u32[]{:S(2)}) copy-start(f32[256,768]{0,1:T(8,128)} %copy.20) | copy-start | bytes 2359300
Sparse Core Ops, SparseCore 0:
  9.5 23.5 all-gather.7
  35.9 96.8 all-gather.3
  134.3 22.6 all-gather.5
  171.7 123.9 all-reduce.8
  299.2 116.8 reduce-scatter.4
  419.0 32.0 reduce-scatter.2
where the time goes:
time: 460 us; the launch traced here: 458 us
  waiting for transfers between devices  377 us (82%)
  matrix products  28.4 us (6%)
  other arithmetic  24.1 us (5%)
  between operations  14.3 us (3%)
  local copies, waits for them, and re-layouts  13.4 us (3%)
    reduce_scatter x1, waiting for transfers between devices, shards(): lax.psum_scatter(make_term(saved_rows, grad_proj).astype(jnp.bfloat16), '...  117 us
    all_gather x1, waiting for transfers between devices, shards(): shard_rows = lax.all_gather(weight_both, 'fs', axis=0, tiled=True)  99.6 us
    psum x1, waiting for transfers between devices, shards(): lax.psum((taps_up_full, taps_gate_full), ('fs', 'tp'))  98.2 us
    reduce_scatter x1, waiting for transfers between devices, shards(): lax.psum_scatter(partial_grad.astype(jnp.bfloat16), 'tp', scatter_dimensi...  31.3 us
    all_gather x1, waiting for transfers between devices, shards(): saved_rows = lax.all_gather(saved_input, 'tp', axis=0, tiled=True)  20.4 us
    unnamed x38, local copies, waits for them, and re-layouts  12.6 us
  transfers between devices with their start and end apart: 6, of which 6 were waited for; matrix products, arithmetic and copies ran while one was open for 11% of the time, Pallas kernels for 0%

commit v1 on v0

v1 whole, which is shorter than its diff:
```python
import functools

import jax
import jax.numpy as jnp
from jax import lax
from jax.experimental import pallas as pl
from jax.experimental.pallas import tpu as pltpu
from jax.sharding import PartitionSpec as P

MESH = pl.DeviceIdType.MESH
F32 = jnp.float32
BF16 = jnp.bfloat16
CORES = 2


def tile_of(extent):
    return 256 if extent % 256 == 0 else 128


def pick(index, table):
    value = jnp.int32(table[0])
    for at in range(1, len(table)):
        value = jnp.where(index == at, jnp.int32(table[at]), value)
    return value


def near_order(z, nz):
    order = [z]
    for step in range(1, nz):
        order += [b for b in (z - step, z + step) if 0 <= b < nz]
    return order


def far_order(z, nz):
    need = {b: (nz - 1 - b) + z if b > z else b + (nz - 1 - z) for b in range(nz) if b != z}
    return sorted(need, key=lambda b: (need[b], -abs(b - z))) + [z]


def delayed(values, steps, row):
    return jnp.where(row >= steps, pltpu.roll(values, steps, 0), 0.0)


def advanced(values, steps, row):
    extent = values.shape[0]
    return jnp.where(row < extent - steps, pltpu.roll(values, extent - steps, 0), 0.0)


def kernel(
    nx, nz, nt,
    later_hbm, saved_hbm, cot_hbm, upw_hbm, gatew_hbm, taps_ref,
    hidden_ref, ingrad_ref, wsum_ref, tapsum_ref,
    weights, rows_l, rows_s, cot, acc_l, acc_s, gproj, gbuf, xrecv, uprecv, dnrecv,
    pbuf, precv, tloc, trecv,
    local_sem, w_recv, w_up, w_dn, w_x, r_recv, r_send, r_fwd,
    x_send, x_recv, up_send, up_recv, dn_send, dn_recv, p_send, p_recv,
    t_send, t_recv, tt_send, tt_recv,
):
    nf = nx * nz
    me = lax.axis_index("fs")
    tp = lax.axis_index("tp")
    x = lax.rem(me, nx)
    z = lax.div(me, nx)
    core = lax.rem(tp, CORES)
    chip = lax.div(tp, CORES)
    chips = nt // CORES
    depth = weights.shape[0] // nf
    both = weights.shape[1]
    cols = both // 2
    seq, width = rows_s.shape
    part = seq // nt

    def remote(src, dst, send, recv, f, t):
        return pltpu.make_async_remote_copy(
            src_ref=src, dst_ref=dst, send_sem=send, recv_sem=recv,
            device_id={"fs": f, "tp": t}, device_id_type=MESH,
        )

    def wblock(b):
        return weights.at[pl.ds(pl.multiple_of(b * depth, depth), depth), :]

    def rblock(ref, t):
        return ref.at[pl.ds(pl.multiple_of(t * part, part), part), :]

    own_w = [
        pltpu.make_async_copy(upw_hbm, wblock(me).at[:, pl.ds(0, cols)], local_sem.at[0]),
        pltpu.make_async_copy(gatew_hbm, wblock(me).at[:, pl.ds(cols, cols)], local_sem.at[1]),
    ]
    own_r = [
        pltpu.make_async_copy(saved_hbm, rblock(rows_s, tp), local_sem.at[2]),
        pltpu.make_async_copy(later_hbm, rblock(rows_l, tp), local_sem.at[3]),
    ]
    own_c = pltpu.make_async_copy(cot_hbm, cot, local_sem.at[4])
    for copy in own_w + own_r + [own_c]:
        copy.start()

    barrier = pltpu.get_barrier_semaphore()
    for d in range(1, nf):
        pl.semaphore_signal(
            barrier, inc=1, device_id={"fs": lax.rem(me + d, nf), "tp": tp}, device_id_type=MESH
        )
    for d in range(1, nt):
        pl.semaphore_signal(
            barrier, inc=1, device_id={"fs": me, "tp": lax.rem(tp + d, nt)}, device_id_type=MESH
        )
    pl.semaphore_wait(barrier, nf - 1 + nt - 1)

    def up_copy(b):
        return remote(wblock(b * nx + x), wblock(b * nx + x), w_up.at[b], w_recv.at[b * nx + x], me + nx, tp)

    def dn_copy(b):
        return remote(wblock(b * nx + x), wblock(b * nx + x), w_dn.at[b], w_recv.at[b * nx + x], me - nx, tp)

    def x_copies(b):
        return [
            remote(
                wblock(b * nx + x), wblock(b * nx + x), w_x.at[d - 1, b],
                w_recv.at[b * nx + x], z * nx + lax.rem(x + d, nx), tp,
            )
            for d in range(1, nx)
        ]

    def w_arrived(b):
        remote(wblock(b), wblock(b), w_up.at[0], w_recv.at[b], me, tp).wait_recv()

    for copy in own_w:
        copy.wait()

    @pl.when(z < nz - 1)
    def _():
        up_copy(z).start()

    @pl.when(z > 0)
    def _():
        dn_copy(z).start()

    for copy in x_copies(z):
        copy.start()

    for copy in own_r:
        copy.wait()
    rows = [rows_s, rows_l]
    mate = chip * CORES + (CORES - 1 - core)

    def row_copy(a, owner, target, sem):
        return remote(rblock(rows[a], owner), rblock(rows[a], owner), sem, r_recv.at[a, owner], me, target)

    def row_arrived(a, owner):
        row_copy(a, owner, tp, r_send.at[0, 0]).wait_recv()

    first_rows = []
    for a in range(2):
        for d in range(1, chips):
            target = lax.rem(chip + d, chips) * CORES + core
            first_rows.append(row_copy(a, tp, target, r_send.at[a, d]))
        first_rows.append(row_copy(a, tp, mate, r_send.at[a, 0]))
    for copy in first_rows:
        copy.start()

    whole = depth % 128 != 0

    def project(b, first=False, size=1):
        rows_of = size * depth
        at = pl.ds(pl.multiple_of(b * depth, rows_of), rows_of)
        step = tile_of(both)

        def body(j, carry):
            tile = pl.ds(pl.multiple_of(j * step, step), step)
            w = weights[at, tile]
            for r, acc in ((rows_s, acc_s), (rows_l, acc_l)):
                term = jnp.dot(r[:, at], w, preferred_element_type=F32)
                if first:
                    acc[:, tile] = term
                else:
                    acc[:, tile] += term
            return carry

        lax.fori_loop(0, both // step, body, 0)

    nears = [near_order(at, nz) for at in range(nz)]
    forwards = []
    for step in range(nz + 1):
        if 0 < step < nz:
            low, high = z - step, z + step

            @pl.when(low >= 0)
            def _():
                w_arrived(low * nx + x)

                @pl.when(z < nz - 1)
                def _():
                    up_copy(low).start()

                for copy in x_copies(low):
                    copy.start()

            @pl.when(high < nz)
            def _():
                w_arrived(high * nx + x)

                @pl.when(z > 0)
                def _():
                    dn_copy(high).start()

                for copy in x_copies(high):
                    copy.start()

        if step == 1:
            for a in range(2):
                for d in range(1, chips):
                    owner = lax.rem(chip + d, chips) * CORES + core
                    row_arrived(a, owner)
                    copy = row_copy(a, owner, mate, r_fwd.at[a, d])
                    copy.start()
                    forwards.append(copy)
            for a in range(2):
                for d in range(chips):
                    row_arrived(a, lax.rem(chip + d, chips) * CORES + (CORES - 1 - core))
            if not whole:
                project(me, first=True)
        if 0 < step < nz and not whole:

            @pl.when(low >= 0)
            def _():
                project(low * nx + x)

            @pl.when(high < nz)
            def _():
                project(high * nx + x)

        if step > 0:
            b = pick(z, [order[step - 1] for order in nears])
            for d in range(1, nx):
                block = b * nx + lax.rem(x + d, nx)
                w_arrived(block)
                if not whole:
                    project(block)
            if whole:
                project(b * nx, first=step == 1, size=nx)

    own_c.wait()
    lanes = 128

    def taps_of(at):
        return [taps_ref[k : k + 1, at] for k in range(3)]

    def conv(values, taps, row):
        return taps[2] * values + taps[1] * delayed(values, 1, row) + taps[0] * delayed(values, 2, row)

    def conv_back(grads, taps, row):
        return taps[2] * grads + taps[1] * advanced(grads, 1, row) + taps[0] * advanced(grads, 2, row)

    tloc[...] = jnp.zeros_like(tloc)

    def backward(j, carry):
        row = lax.broadcasted_iota(jnp.int32, (seq, lanes), 0)
        at_u = pl.ds(pl.multiple_of(j * lanes, lanes), lanes)
        at_g = pl.ds(pl.multiple_of(cols + j * lanes, lanes), lanes)
        tu, tg = taps_of(at_u), taps_of(at_g)
        vu = acc_s[:, at_u].astype(BF16).astype(F32)
        vg = acc_s[:, at_g].astype(BF16).astype(F32)
        cu, cg = conv(vu, tu, row), conv(vg, tg, row)
        sig = jax.nn.sigmoid(cg)
        upstream = cot[:, at_u].astype(F32)
        gu = upstream * (cg * sig)
        gg = upstream * cu * sig * (1.0 + cg * (1.0 - sig))
        gproj[:, at_u] = conv_back(gu, tu, row).astype(BF16)
        gproj[:, at_g] = conv_back(gg, tg, row).astype(BF16)
        for at, g, v in ((at_u, gu, vu), (at_g, gg, vg)):
            tloc[0:1, at] = jnp.sum(g * delayed(v, 2, row), axis=0, keepdims=True)
            tloc[1:2, at] = jnp.sum(g * delayed(v, 1, row), axis=0, keepdims=True)
            tloc[2:3, at] = jnp.sum(g * v, axis=0, keepdims=True)
        return carry

    lax.fori_loop(0, cols // lanes, backward, 0)

    def weight_term(b, size=1):
        rows_of = size * depth
        left = rows_s[:, pl.ds(pl.multiple_of(b * depth, rows_of), rows_of)].T
        step = tile_of(both)

        def body(j, carry):
            tile = pl.ds(pl.multiple_of(j * step, step), step)
            term = jnp.dot(left, gproj[:, tile], preferred_element_type=F32).astype(BF16)
            for i in range(size):
                gbuf[b + i, :, tile] = term[i * depth : (i + 1) * depth]
            return carry

        lax.fori_loop(0, both // step, body, 0)

    fars = [far_order(at, nz) for at in range(nz)]
    order = [pick(z, [o[q] for o in fars]) for q in range(nz)]

    def x_grad(b, d):
        to = lax.rem(x + d, nx)
        return remote(
            gbuf.at[b * nx + to], xrecv.at[d - 1, b], x_send.at[d - 1, b], x_recv.at[d - 1, b],
            z * nx + to, tp,
        )

    for q in range(nz):
        if whole:
            weight_term(order[q] * nx, size=nx)
        for d in range(1, nx):
            if not whole:
                weight_term(order[q] * nx + lax.rem(x + d, nx))
            x_grad(order[q], d).start()

    def tap_copy(d):
        return remote(
            tloc, trecv.at[d - 1], t_send.at[d - 1], t_recv.at[d - 1], lax.rem(me + d, nf), tp
        )

    for d in range(1, nf):
        tap_copy(d).start()

    def input_term(t):
        at = pl.ds(pl.multiple_of(t * part, part), part)
        step = tile_of(width)

        def body(j, carry):
            tile = pl.ds(pl.multiple_of(j * step, step), step)
            term = lax.dot_general(
                gproj[at, :], weights[tile, :], (((1,), (1,)), ((), ())), preferred_element_type=F32
            )
            pbuf[t, :, tile] = term.astype(BF16)
            return carry

        lax.fori_loop(0, width // step, body, 0)

    def part_copy(d):
        to = lax.rem(tp + d, nt)
        return remote(pbuf.at[to], precv.at[d - 1], p_send.at[d - 1], p_recv.at[d - 1], me, to)

    for d in range(1, nt):
        input_term(lax.rem(tp + d, nt))
        part_copy(d).start()
    for q in range(nz):
        if not whole:
            weight_term(order[q] * nx + x)
    input_term(tp)

    def forward(j, carry):
        row = lax.broadcasted_iota(jnp.int32, (seq, lanes), 0)
        at_u = pl.ds(pl.multiple_of(j * lanes, lanes), lanes)
        at_g = pl.ds(pl.multiple_of(cols + j * lanes, lanes), lanes)
        cu = conv(acc_l[:, at_u].astype(BF16).astype(F32), taps_of(at_u), row)
        cg = conv(acc_l[:, at_g].astype(BF16).astype(F32), taps_of(at_g), row)
        hidden_ref[:, at_u] = (cg * jax.nn.sigmoid(cg) * cu).astype(BF16)
        return carry

    lax.fori_loop(0, cols // lanes, forward, 0)

    total = tloc[...]
    for d in range(1, nf):
        tap_copy(d).wait_recv()
        total = total + trecv[d - 1]
    tapsum_ref[tp] = total

    def tap_full(d):
        return remote(
            tapsum_ref.at[tp], tapsum_ref.at[tp], tt_send.at[d - 1], tt_recv.at[tp],
            me, lax.rem(tp + d, nt),
        )

    for d in range(1, nt):
        tap_full(d).start()

    def add_into(b, sources):
        value = gbuf[b].astype(F32)
        for source in sources:
            value = value + source[...].astype(F32)
        gbuf[b] = value.astype(BF16)

    def up_grad(b):
        return remote(gbuf.at[b * nx + x], uprecv.at[b], up_send.at[b], up_recv.at[b], me + nx, tp)

    def dn_grad(b):
        return remote(gbuf.at[b * nx + x], dnrecv.at[b], dn_send.at[b], dn_recv.at[b], me - nx, tp)

    for q in range(nz):
        b = order[q]
        mine = b * nx + x
        for d in range(1, nx):
            x_grad(b, d).wait_recv()
        if q < nz - 1:
            fed = jnp.logical_or(jnp.logical_and(b > z, z > 0), jnp.logical_and(b < z, z < nz - 1))

            @pl.when(jnp.logical_and(b > z, z > 0))
            def _():
                up_grad(b).wait_recv()
                add_into(mine, [xrecv.at[d - 1, b] for d in range(1, nx)] + [uprecv.at[b]])

            @pl.when(jnp.logical_and(b < z, z < nz - 1))
            def _():
                dn_grad(b).wait_recv()
                add_into(mine, [xrecv.at[d - 1, b] for d in range(1, nx)] + [dnrecv.at[b]])

            @pl.when(jnp.logical_not(fed))
            def _():
                add_into(mine, [xrecv.at[d - 1, b] for d in range(1, nx)])

            @pl.when(b > z)
            def _():
                up_grad(b).start()

            @pl.when(b < z)
            def _():
                dn_grad(b).start()

        else:
            value = gbuf[mine].astype(F32)
            for d in range(1, nx):
                value = value + xrecv[d - 1, b].astype(F32)
            wsum_ref[...] = value

            @pl.when(z > 0)
            def _():
                up_grad(b).wait_recv()
                wsum_ref[...] += uprecv[b].astype(F32)

            @pl.when(z < nz - 1)
            def _():
                dn_grad(b).wait_recv()
                wsum_ref[...] += dnrecv[b].astype(F32)

    total = pbuf[tp].astype(F32)
    for d in range(1, nt):
        part_copy(d).wait_recv()
        total = total + precv[d - 1].astype(F32)
    ingrad_ref[...] = total.astype(BF16)

    for d in range(1, nt):
        remote(
            tapsum_ref.at[tp], tapsum_ref.at[lax.rem(tp + d, nt)], tt_send.at[d - 1],
            tt_recv.at[lax.rem(tp + d, nt)], me, lax.rem(tp + d, nt),
        ).wait_recv()
        tap_full(d).wait_send()
        part_copy(d).wait_send()
    for d in range(1, nf):
        tap_copy(d).wait_send()
    for copy in first_rows + forwards:
        copy.wait_send()
    for b in range(nz):
        for copy in x_copies(b):
            copy.wait_send()
        for d in range(1, nx):
            x_grad(b, d).wait_send()

        @pl.when(jnp.logical_and(z < nz - 1, b <= z))
        def _():
            up_copy(b).wait_send()

        @pl.when(jnp.logical_and(z > 0, b >= z))
        def _():
            dn_copy(b).wait_send()

        @pl.when(b > z)
        def _():
            up_grad(b).wait_send()

        @pl.when(b < z)
        def _():
            dn_grad(b).wait_send()


def shards(
    nf, nt,
    later_input, saved_input, cotangent, up_weight, gate_weight,
    up_taps, gate_taps, up_grad_sum, gate_grad_sum, up_taps_sum, gate_taps_sum,
):
    nx = 1 << ((nf.bit_length() - 1) // 2)
    nz = nf // nx
    depth, cols = up_weight.shape
    both = 2 * cols
    part, width = later_input.shape
    seq = part * nt
    tokens_all = part * nf * nt
    grad_scale = jnp.float32(tokens_all ** (-0.5))
    offset = lax.axis_index("tp") * cols
    taps_both = jnp.concatenate(
        [
            lax.dynamic_slice_in_dim(up_taps, offset, cols, 1),
            lax.dynamic_slice_in_dim(gate_taps, offset, cols, 1),
        ],
        axis=1,
    ).astype(F32)
    dma = pltpu.SemaphoreType.DMA
    vmem = pl.BlockSpec(memory_space=pltpu.VMEM)
    hbm = pl.BlockSpec(memory_space=pl.ANY)
    hidden, input_grad, weight_grad, taps_sum = pl.pallas_call(
        functools.partial(kernel, nx, nz, nt),
        out_shape=(
            jax.ShapeDtypeStruct((seq, cols), BF16),
            jax.ShapeDtypeStruct((part, width), BF16),
            jax.ShapeDtypeStruct((depth, both), F32),
            jax.ShapeDtypeStruct((nt, 8, both), F32),
        ),
        in_specs=[hbm] * 5 + [vmem],
        out_specs=(vmem,) * 4,
        scratch_shapes=[
            pltpu.VMEM((width, both), BF16),
            pltpu.VMEM((seq, width), BF16),
            pltpu.VMEM((seq, width), BF16),
            pltpu.VMEM((seq, cols), BF16),
            pltpu.VMEM((seq, both), F32),
            pltpu.VMEM((seq, both), F32),
            pltpu.VMEM((seq, both), BF16),
            pltpu.VMEM((nf, depth, both), BF16),
            pltpu.VMEM((nx - 1, nz, depth, both), BF16),
            pltpu.VMEM((nz, depth, both), BF16),
            pltpu.VMEM((nz, depth, both), BF16),
            pltpu.VMEM((nt, part, width), BF16),
            pltpu.VMEM((nt - 1, part, width), BF16),
            pltpu.VMEM((8, both), F32),
            pltpu.VMEM((nf - 1, 8, both), F32),
            dma((5,)),
            dma((nf,)),
            dma((nz,)),
            dma((nz,)),
            dma((nx - 1, nz)),
            dma((2, nt)),
            dma((2, nt)),
            dma((2, nt)),
            dma((nx - 1, nz)),
            dma((nx - 1, nz)),
            dma((nz,)),
            dma((nz,)),
            dma((nz,)),
            dma((nz,)),
            dma((nt - 1,)),
            dma((nt - 1,)),
            dma((nf - 1,)),
            dma((nf - 1,)),
            dma((nt - 1,)),
            dma((nt,)),
        ],
        compiler_params=pltpu.CompilerParams(
            collective_id=0, has_side_effects=True, vmem_limit_bytes=67043328
        ),
        name="layer",
    )(later_input, saved_input, cotangent, up_weight, gate_weight, taps_both)
    new_up_sum = up_grad_sum + grad_scale * weight_grad[:, :cols]
    new_gate_sum = gate_grad_sum + grad_scale * weight_grad[:, cols:]
    taps_up = taps_sum[:, :3, :cols].transpose(1, 0, 2).reshape(3, nt * cols)
    taps_gate = taps_sum[:, :3, cols:].transpose(1, 0, 2).reshape(3, nt * cols)
    new_up_taps_sum = up_taps_sum + grad_scale * taps_up
    new_gate_taps_sum = gate_taps_sum + grad_scale * taps_gate
    return (hidden, input_grad, new_up_sum, new_gate_sum, new_up_taps_sum, new_gate_taps_sum)


def solution(mesh):
    return jax.shard_map(
        functools.partial(shards, mesh.shape["fs"], mesh.shape["tp"]),
        mesh=mesh,
        in_specs=(
            P(("fs", "tp"), None),
            P(("fs", "tp"), None),
            P("fs", "tp"),
            P("fs", "tp"),
            P("fs", "tp"),
            P(),
            P(),
            P("fs", "tp"),
            P("fs", "tp"),
            P(),
            P(),
        ),
        out_specs=(P("fs", "tp"), P(("fs", "tp"), None), P("fs", "tp"), P("fs", "tp"), P(), P()),
        check_vma=False,
    )
```

time: 460 us -> 219 us (0.48)
  the two profiles are of different devices: /device:TPU:24 before, /device:TPU:10 now
where the time goes in v1:
time: 219 us; the launch traced here: 218 us
  Pallas kernels  207 us (95%)
  other arithmetic  7.69 us (4%)
  local copies, waits for them, and re-layouts  2.84 us (1%)
    pallas_call x1, Pallas kernels, shards(): pl.pallas_call(functools.partial(kernel, nx, nz, nt), out_shape=(jax.Shap...  207 us

profile of v1, /device:TPU:10, one launch (start us, length us, event | category | flops | bytes accessed | tf_op | source)
XLA Modules:
  0.0 218.1 jit_solution(12324747529383021074)
XLA Ops:
  0.6 0.7 constant_dynamic-slice_fusion
  1.4 0.6 maximum_convert_fusion.taps_ref
  2.0 206.9 %layer.1 = (bf16[512,768]{1,0:T(8,128)(2,1)}, bf16[128,2048]{1,0:T(8,128)(2,1)}, f32[256,1536]{1,0:T(8,128)}, f32[4,8,1536]{2,1,0:T(8,128)}) custom-call(bf16[128,2048]{1,0:T(8,128)(2,1)} %later_hbm.1, bf16[128,2048]{1,0:T(8,128)(2,1)} %saved_hbm.1, bf16[512,768]{1,0:T(8,128)(2,1)} %cot_hbm.1, bf16[256,768]{1,0:T(8,128)(2,1)} %upw_hbm.1, ...), custom_call_target="tpu_custom_call" | custom-call | tf_op jit(solution)/shard_map/layer/pallas_call | solution.py:490
  208.9 1.0 slice_multiply_fusion
  209.9 1.4 add.20
  211.3 1.4 add.19
  212.7 0.0 copy-start
  212.7 3.2 %multiply_add_fusion = (f32[256,768]{1,0:T(8,128)}, f32[256,768]{1,0:T(8,128)}) fusion(f32[256,768]{1,0:T(8,128)} %param.19, f32[256,1536]{1,0:T(8,128)} %get-tuple-element.12, f32[256,768]{1,0:T(8,128)} %param.18), kind=kLoop, calls=%fused_computation | loop fusion | flops 786432 | bytes 4718592 | tf_op jit(solution)/shard_map/add | solution.py:543
  216.0 0.0 copy-start.1
  216.0 0.0 copy-done
  216.0 0.9 copy.19
  216.9 0.4 copy-done.1
  217.3 0.8 copy.20
Async XLA Ops:
  212.7 3.3 %copy-start = (bf16[512,768]{1,0:T(8,128)(2,1)S(1)}, bf16[512,768]{1,0:T(8,128)(2,1)}, u32[]{:S(2)}) copy-start(bf16[512,768]{1,0:T(8,128)(2,1)} %get-tuple-element.26) | copy-start | bytes 2359300
  216.0 1.3 copy-start.1

commit v2 on v1

--- a/solution.py
+++ b/solution.py
@@ -46,14 +46,15 @@
 
 
 def kernel(
-    nx, nz, nt,
-    later_hbm, saved_hbm, cot_hbm, upw_hbm, gatew_hbm, taps_ref,
-    hidden_ref, ingrad_ref, wsum_ref, tapsum_ref,
+    nx, nz, nt, scale,
+    later_hbm, saved_hbm, cot_hbm, upw_hbm, gatew_hbm, upsum_hbm, gatesum_hbm,
+    uptaps_ref, gatetaps_ref, uptsum_ref, gatetsum_ref,
+    hidden_ref, ingrad_ref, newup_ref, newgate_ref, newupt_ref, newgatet_ref,
     weights, rows_l, rows_s, cot, acc_l, acc_s, gproj, gbuf, xrecv, uprecv, dnrecv,
-    pbuf, precv, tloc, trecv,
+    pbuf, precv, oldsum, taps, tloc, trecv, tzrecv, tapsum,
     local_sem, w_recv, w_up, w_dn, w_x, r_recv, r_send, r_fwd,
     x_send, x_recv, up_send, up_recv, dn_send, dn_recv, p_send, p_recv,
-    t_send, t_recv, tt_send, tt_recv,
+    t_send, t_recv, tz_send, tz_recv, tt_send, tt_recv,
 ):
     nf = nx * nz
     me = lax.axis_index("fs")
@@ -90,7 +91,11 @@
         pltpu.make_async_copy(later_hbm, rblock(rows_l, tp), local_sem.at[3]),
     ]
     own_c = pltpu.make_async_copy(cot_hbm, cot, local_sem.at[4])
-    for copy in own_w + own_r + [own_c]:
+    own_s = [
+        pltpu.make_async_copy(upsum_hbm, oldsum.at[0], local_sem.at[5]),
+        pltpu.make_async_copy(gatesum_hbm, oldsum.at[1], local_sem.at[6]),
+    ]
+    for copy in own_w + own_r + [own_c] + own_s:
         copy.start()
 
     barrier = pltpu.get_barrier_semaphore()
@@ -240,8 +245,12 @@
     own_c.wait()
     lanes = 128
 
+    tap_lanes = pl.ds(pl.multiple_of(tp * cols, 128), cols)
+    taps[0:3, 0:cols] = uptaps_ref[:, tap_lanes].astype(F32)
+    taps[0:3, cols:both] = gatetaps_ref[:, tap_lanes].astype(F32)
+
     def taps_of(at):
-        return [taps_ref[k : k + 1, at] for k in range(3)]
+        return [taps[k : k + 1, at] for k in range(3)]
 
     def conv(values, taps, row):
         return taps[2] * values + taps[1] * delayed(values, 1, row) + taps[0] * delayed(values, 2, row)
@@ -265,10 +274,10 @@
         gg = upstream * cu * sig * (1.0 + cg * (1.0 - sig))
         gproj[:, at_u] = conv_back(gu, tu, row).astype(BF16)
         gproj[:, at_g] = conv_back(gg, tg, row).astype(BF16)
-        for at, g, v in ((at_u, gu, vu), (at_g, gg, vg)):
-            tloc[0:1, at] = jnp.sum(g * delayed(v, 2, row), axis=0, keepdims=True)
-            tloc[1:2, at] = jnp.sum(g * delayed(v, 1, row), axis=0, keepdims=True)
-            tloc[2:3, at] = jnp.sum(g * v, axis=0, keepdims=True)
+        for k, g, v in ((0, gu, vu), (3, gg, vg)):
+            tloc[k : k + 1, at_u] = jnp.sum(g * delayed(v, 2, row), axis=0, keepdims=True)
+            tloc[k + 1 : k + 2, at_u] = jnp.sum(g * delayed(v, 1, row), axis=0, keepdims=True)
+            tloc[k + 2 : k + 3, at_u] = jnp.sum(g * v, axis=0, keepdims=True)
         return carry
 
     lax.fori_loop(0, cols // lanes, backward, 0)
@@ -296,6 +305,14 @@
             gbuf.at[b * nx + to], xrecv.at[d - 1, b], x_send.at[d - 1, b], x_recv.at[d - 1, b],
             z * nx + to, tp,
         )
+
+    def tap_x(d):
+        return remote(
+            tloc, trecv.at[d - 1], t_send.at[d - 1], t_recv.at[d - 1], z * nx + lax.rem(x + d, nx), tp
+        )
+
+    for d in range(1, nx):
+        tap_x(d).start()
 
     for q in range(nz):
         if whole:
@@ -304,14 +321,6 @@
             if not whole:
                 weight_term(order[q] * nx + lax.rem(x + d, nx))
             x_grad(order[q], d).start()
-
-    def tap_copy(d):
-        return remote(
-            tloc, trecv.at[d - 1], t_send.at[d - 1], t_recv.at[d - 1], lax.rem(me + d, nf), tp
-        )
-
-    for d in range(1, nf):
-        tap_copy(d).start()
 
     def input_term(t):
         at = pl.ds(pl.multiple_of(t * part, part), part)
@@ -351,19 +360,24 @@
     lax.fori_loop(0, cols // lanes, forward, 0)
 
     total = tloc[...]
-    for d in range(1, nf):
-        tap_copy(d).wait_recv()
+    for d in range(1, nx):
+        tap_x(d).wait_recv()
         total = total + trecv[d - 1]
-    tapsum_ref[tp] = total
+    tzrecv[nz - 1] = total
+
+    def tap_z(d):
+        return remote(
+            tzrecv.at[nz - 1], tzrecv.at[d - 1], tz_send.at[d - 1], tz_recv.at[d - 1],
+            lax.rem(z + d, nz) * nx + x, tp,
+        )
 
     def tap_full(d):
         return remote(
-            tapsum_ref.at[tp], tapsum_ref.at[tp], tt_send.at[d - 1], tt_recv.at[tp],
-            me, lax.rem(tp + d, nt),
+            tapsum.at[tp], tapsum.at[tp], tt_send.at[d - 1], tt_recv.at[tp], me, lax.rem(tp + d, nt)
         )
 
-    for d in range(1, nt):
-        tap_full(d).start()
+    for d in range(1, nz):
+        tap_z(d).start()
 
     def add_into(b, sources):
         value = gbuf[b].astype(F32)
@@ -408,20 +422,35 @@
                 dn_grad(b).start()
 
         else:
-            value = gbuf[mine].astype(F32)
-            for d in range(1, nx):
-                value = value + xrecv[d - 1, b].astype(F32)
-            wsum_ref[...] = value
+            for copy in own_s:
+                copy.wait()
+            halves = ((newup_ref, 0, pl.ds(0, cols)), (newgate_ref, 1, pl.ds(cols, cols)))
+            for new, at, lane in halves:
+                value = gbuf[mine, :, lane].astype(F32)
+                for d in range(1, nx):
+                    value = value + xrecv[d - 1, b, :, lane].astype(F32)
+                new[...] = oldsum[at] + scale * value
 
             @pl.when(z > 0)
             def _():
                 up_grad(b).wait_recv()
-                wsum_ref[...] += uprecv[b].astype(F32)
+                for new, at, lane in halves:
+                    new[...] += scale * uprecv[b, :, lane].astype(F32)
 
             @pl.when(z < nz - 1)
             def _():
                 dn_grad(b).wait_recv()
-                wsum_ref[...] += dnrecv[b].astype(F32)
+                for new, at, lane in halves:
+                    new[...] += scale * dnrecv[b, :, lane].astype(F32)
+
+        if q == 0:
+            total = tzrecv[nz - 1]
+            for d in range(1, nz):
+                tap_z(d).wait_recv()
+                total = total + tzrecv[d - 1]
+            tapsum[tp] = total
+            for d in range(1, nt):
+                tap_full(d).start()
 
     total = pbuf[tp].astype(F32)
     for d in range(1, nt):
@@ -430,14 +459,20 @@
     ingrad_ref[...] = total.astype(BF16)
 
     for d in range(1, nt):
+        from_tp = lax.rem(tp + d, nt)
         remote(
-            tapsum_ref.at[tp], tapsum_ref.at[lax.rem(tp + d, nt)], tt_send.at[d - 1],
-            tt_recv.at[lax.rem(tp + d, nt)], me, lax.rem(tp + d, nt),
+            tapsum.at[tp], tapsum.at[from_tp], tt_send.at[d - 1], tt_recv.at[from_tp], me, from_tp
         ).wait_recv()
         tap_full(d).wait_send()
         part_copy(d).wait_send()
-    for d in range(1, nf):
-        tap_copy(d).wait_send()
+    for t in range(nt):
+        lane = pl.ds(t * cols, cols)
+        newupt_ref[:, lane] = uptsum_ref[:, lane] + scale * tapsum[t, 0:3]
+        newgatet_ref[:, lane] = gatetsum_ref[:, lane] + scale * tapsum[t, 3:6]
+    for d in range(1, nx):
+        tap_x(d).wait_send()
+    for d in range(1, nz):
+        tap_z(d).wait_send()
     for copy in first_rows + forwards:
         copy.wait_send()
     for b in range(nz):
@@ -474,29 +509,23 @@
     both = 2 * cols
     part, width = later_input.shape
     seq = part * nt
-    tokens_all = part * nf * nt
-    grad_scale = jnp.float32(tokens_all ** (-0.5))
-    offset = lax.axis_index("tp") * cols
-    taps_both = jnp.concatenate(
-        [
-            lax.dynamic_slice_in_dim(up_taps, offset, cols, 1),
-            lax.dynamic_slice_in_dim(gate_taps, offset, cols, 1),
-        ],
-        axis=1,
-    ).astype(F32)
+    scale = float(part * nf * nt) ** (-0.5)
+    total_cols = up_taps.shape[1]
     dma = pltpu.SemaphoreType.DMA
     vmem = pl.BlockSpec(memory_space=pltpu.VMEM)
     hbm = pl.BlockSpec(memory_space=pl.ANY)
-    hidden, input_grad, weight_grad, taps_sum = pl.pallas_call(
-        functools.partial(kernel, nx, nz, nt),
+    return pl.pallas_call(
+        functools.partial(kernel, nx, nz, nt, scale),
         out_shape=(
             jax.ShapeDtypeStruct((seq, cols), BF16),
             jax.ShapeDtypeStruct((part, width), BF16),
-            jax.ShapeDtypeStruct((depth, both), F32),
-            jax.ShapeDtypeStruct((nt, 8, both), F32),
+            jax.ShapeDtypeStruct((depth, cols), F32),
+            jax.ShapeDtypeStruct((depth, cols), F32),
+            jax.ShapeDtypeStruct((3, total_cols), F32),
+            jax.ShapeDtypeStruct((3, total_cols), F32),
         ),
-        in_specs=[hbm] * 5 + [vmem],
-        out_specs=(vmem,) * 4,
+        in_specs=[hbm] * 7 + [vmem] * 4,
+        out_specs=(vmem,) * 6,
         scratch_shapes=[
             pltpu.VMEM((width, both), BF16),
             pltpu.VMEM((seq, width), BF16),
@@ -511,9 +540,13 @@
             pltpu.VMEM((nz, depth, both), BF16),
             pltpu.VMEM((nt, part, width), BF16),
             pltpu.VMEM((nt - 1, part, width), BF16),
+            pltpu.VMEM((2, depth, cols), F32),
             pltpu.VMEM((8, both), F32),
-            pltpu.VMEM((nf - 1, 8, both), F32),
-            dma((5,)),
+            pltpu.VMEM((8, cols), F32),
+            pltpu.VMEM((nx - 1, 8, cols), F32),
+            pltpu.VMEM((nz, 8, cols), F32),
+            pltpu.VMEM((nt, 8, cols), F32),
+            dma((7,)),
             dma((nf,)),
             dma((nz,)),
             dma((nz,)),
@@ -529,8 +562,10 @@
             dma((nz,)),
             dma((nt - 1,)),
             dma((nt - 1,)),
-            dma((nf - 1,)),
-            dma((nf - 1,)),
+            dma((nx - 1,)),
+            dma((nx - 1,)),
+            dma((nz - 1,)),
+            dma((nz - 1,)),
             dma((nt - 1,)),
             dma((nt,)),
         ],
@@ -538,14 +573,10 @@
             collective_id=0, has_side_effects=True, vmem_limit_bytes=67043328
         ),
         name="layer",
-    )(later_input, saved_input, cotangent, up_weight, gate_weight, taps_both)
-    new_up_sum = up_grad_sum + grad_scale * weight_grad[:, :cols]
-    new_gate_sum = gate_grad_sum + grad_scale * weight_grad[:, cols:]
-    taps_up = taps_sum[:, :3, :cols].transpose(1, 0, 2).reshape(3, nt * cols)
-    taps_gate = taps_sum[:, :3, cols:].transpose(1, 0, 2).reshape(3, nt * cols)
-    new_up_taps_sum = up_taps_sum + grad_scale * taps_up
-    new_gate_taps_sum = gate_taps_sum + grad_scale * taps_gate
-    return (hidden, input_grad, new_up_sum, new_gate_sum, new_up_taps_sum, new_gate_taps_sum)
+    )(
+        later_input, saved_input, cotangent, up_weight, gate_weight, up_grad_sum, gate_grad_sum,
+        up_taps, gate_taps, up_taps_sum, gate_taps_sum,
+    )
 
 
 def solution(mesh):

time: 219 us -> 171 us (0.78)
  the two profiles are of different devices: /device:TPU:10 before, /device:TPU:8 now
where the time goes in v2:
time: 171 us; the launch traced here: 170 us
  Pallas kernels  163 us (95%)
  local copies, waits for them, and re-layouts  7.18 us (4%)
    pallas_call x1, Pallas kernels, shards(): pl.pallas_call(functools.partial(kernel, nx, nz, nt, scale), out_shape=(j...  163 us
    unnamed x16, local copies, waits for them, and re-layouts  7.18 us

profile of v2, /device:TPU:8, one launch (start us, length us, event | category | flops | bytes accessed | tf_op | source)
XLA Modules:
  0.0 170.5 jit_solution(11775777734811208786)
XLA Ops:
  0.6 162.7 %layer.1 = (bf16[512,768]{1,0:T(8,128)(2,1)}, bf16[128,2048]{1,0:T(8,128)(2,1)}, f32[256,768]{1,0:T(8,128)}, f32[256,768]{1,0:T(8,128)}, f32[3,3072]{1,0:T(4,128)}, /*index=5*/f32[3,3072]{1,0:T(4,128)}) custom-call(bf16[128,2048]{1,0:T(8,128)(2,1)} %later_hbm.1, bf16[128,2048]{1,0:T(8,128)(2,1)} %saved_hbm.1, bf16[512,768]{1,0:T(8,128)(2,1)} %cot_hbm.1, ...), custom_call_target="tpu_custom_call" | custom-call | tf_op jit(solution)/shard_map/layer/pallas_call | solution.py:517
  163.3 0.0 copy-start.2
  163.3 2.1 %copy.23 = bf16[512,768]{1,0:T(8,128)(2,1)} copy(bf16[512,768]{1,0:T(8,128)(2,1)} %get-tuple-element.12) | data formatting | bytes 1572864
  165.4 0.0 copy-done.2
  165.4 0.0 copy-start.1
  165.4 0.8 copy.24
  166.2 0.5 copy-done.1
  166.8 0.0 copy-start
  166.8 0.9 copy.25
  167.6 0.5 copy-done
  168.2 0.0 copy-start.4
  168.2 0.9 copy.26
  169.1 0.0 copy-done.4
  169.1 0.0 copy-start.3
  169.1 0.6 copy.27
  169.7 0.2 copy-done.3
  169.9 0.6 copy.28
Async XLA Ops:
  163.3 2.1 %copy-start.2 = (bf16[128,2048]{1,0:T(8,128)(2,1)S(1)}, bf16[128,2048]{1,0:T(8,128)(2,1)}, u32[]{:S(2)}) copy-start(bf16[128,2048]{1,0:T(8,128)(2,1)} %get-tuple-element.13) | copy-start | bytes 1572868
  165.4 1.3 copy-start.1
  166.8 1.4 copy-start
  168.2 0.9 copy-start.4
  169.1 0.8 copy-start.3

commit v3 on v2

--- a/solution.py
+++ b/solution.py
@@ -25,10 +25,11 @@
 
 
 def near_order(z, nz):
+    pair = z ^ 1
     order = [z]
     for step in range(1, nz):
-        order += [b for b in (z - step, z + step) if 0 <= b < nz]
-    return order
+        order += [b for b in (z - step, z + step) if 0 <= b < nz and b != pair]
+    return order + [pair]
 
 
 def far_order(z, nz):
@@ -51,9 +52,9 @@
     uptaps_ref, gatetaps_ref, uptsum_ref, gatetsum_ref,
     hidden_ref, ingrad_ref, newup_ref, newgate_ref, newupt_ref, newgatet_ref,
     weights, rows_l, rows_s, cot, acc_l, acc_s, gproj, gbuf, xrecv, uprecv, dnrecv,
-    pbuf, precv, oldsum, taps, tloc, trecv, tzrecv, tapsum,
-    local_sem, w_recv, w_up, w_dn, w_x, r_recv, r_send, r_fwd,
-    x_send, x_recv, up_send, up_recv, dn_send, dn_recv, p_send, p_recv,
+    swrecv, pbuf, precv, oldsum, taps, tloc, trecv, tzrecv, tapsum,
+    local_sem, w_recv, w_up, w_dn, w_x, w_swap, r_recv, r_send, r_fwd,
+    x_send, x_recv, sw_send, sw_recv, up_send, up_recv, dn_send, dn_recv, p_send, p_recv,
     t_send, t_recv, tz_send, tz_recv, tt_send, tt_recv,
 ):
     nf = nx * nz
@@ -64,11 +65,13 @@
     core = lax.rem(tp, CORES)
     chip = lax.div(tp, CORES)
     chips = nt // CORES
+    pair = z + 1 - 2 * lax.rem(z, 2)
     depth = weights.shape[0] // nf
     both = weights.shape[1]
     cols = both // 2
     seq, width = rows_s.shape
     part = seq // nt
+    half = depth // 2
 
     def remote(src, dst, send, recv, f, t):
         return pltpu.make_async_remote_copy(
@@ -109,37 +112,56 @@
         )
     pl.semaphore_wait(barrier, nf - 1 + nt - 1)
 
-    def up_copy(b):
-        return remote(wblock(b * nx + x), wblock(b * nx + x), w_up.at[b], w_recv.at[b * nx + x], me + nx, tp)
-
-    def dn_copy(b):
-        return remote(wblock(b * nx + x), wblock(b * nx + x), w_dn.at[b], w_recv.at[b * nx + x], me - nx, tp)
-
-    def x_copies(b):
+    def whalf(b, i):
+        return weights.at[pl.ds(pl.multiple_of(b * depth + i * half, half), half), :]
+
+    def w_copy(b, i, send, f):
+        return remote(whalf(b, i), whalf(b, i), send, w_recv.at[b, i], f, tp)
+
+    def up_copy(b, i):
+        return w_copy(b * nx + x, i, w_up.at[b, i], me + nx)
+
+    def dn_copy(b, i):
+        return w_copy(b * nx + x, i, w_dn.at[b, i], me - nx)
+
+    def x_copies(b, i):
         return [
-            remote(
-                wblock(b * nx + x), wblock(b * nx + x), w_x.at[d - 1, b],
-                w_recv.at[b * nx + x], z * nx + lax.rem(x + d, nx), tp,
-            )
+            w_copy(b * nx + x, i, w_x.at[d - 1, b, i], z * nx + lax.rem(x + d, nx))
             for d in range(1, nx)
         ]
 
-    def w_arrived(b):
-        remote(wblock(b), wblock(b), w_up.at[0], w_recv.at[b], me, tp).wait_recv()
+    def swap_copy(d):
+        return w_copy(z * nx + lax.rem(x + d, nx), 1, w_swap.at[d - 1], pair * nx + x)
+
+    def pass_x(b, i):
+        if i == 0:
+            for copy in x_copies(b, i):
+                copy.start()
+        else:
+
+            @pl.when(b != pair)
+            def _():
+                for copy in x_copies(b, i):
+                    copy.start()
+
+    def w_arrived(b, i):
+        w_copy(b, i, w_up.at[0, 0], me).wait_recv()
 
     for copy in own_w:
         copy.wait()
 
-    @pl.when(z < nz - 1)
-    def _():
-        up_copy(z).start()
-
-    @pl.when(z > 0)
-    def _():
-        dn_copy(z).start()
-
-    for copy in x_copies(z):
-        copy.start()
+    for i in range(2):
+
+        @pl.when(z < nz - 1)
+        def _():
+            up_copy(z, i).start()
+
+        @pl.when(z > 0)
+        def _():
+            dn_copy(z, i).start()
+
+        for copy in x_copies(z, i):
+            copy.start()
 
     for copy in own_r:
         copy.wait()
@@ -163,7 +185,7 @@
 
     whole = depth % 128 != 0
 
-    def project(b, first=False, size=1):
+    def project(b, first=False, size=1, which=(0, 1)):
         rows_of = size * depth
         at = pl.ds(pl.multiple_of(b * depth, rows_of), rows_of)
         step = tile_of(both)
@@ -171,7 +193,8 @@
         def body(j, carry):
             tile = pl.ds(pl.multiple_of(j * step, step), step)
             w = weights[at, tile]
-            for r, acc in ((rows_s, acc_s), (rows_l, acc_l)):
+            for a in which:
+                r, acc = ((rows_s, acc_s), (rows_l, acc_l))[a]
                 term = jnp.dot(r[:, at], w, preferred_element_type=F32)
                 if first:
                     acc[:, tile] = term
@@ -187,27 +210,27 @@
         if 0 < step < nz:
             low, high = z - step, z + step
 
-            @pl.when(low >= 0)
-            def _():
-                w_arrived(low * nx + x)
-
-                @pl.when(z < nz - 1)
+            for i in range(2):
+
+                @pl.when(low >= 0)
                 def _():
-                    up_copy(low).start()
-
-                for copy in x_copies(low):
-                    copy.start()
-
-            @pl.when(high < nz)
-            def _():
-                w_arrived(high * nx + x)
-
-                @pl.when(z > 0)
+                    w_arrived(low * nx + x, i)
+
+                    @pl.when(z < nz - 1)
+                    def _():
+                        up_copy(low, i).start()
+
+                    pass_x(low, i)
+
+                @pl.when(high < nz)
                 def _():
-                    dn_copy(high).start()
-
-                for copy in x_copies(high):
-                    copy.start()
+                    w_arrived(high * nx + x, i)
+
+                    @pl.when(z > 0)
+                    def _():
+                        dn_copy(high, i).start()
+
+                    pass_x(high, i)
 
         if step == 1:
             for a in range(2):
@@ -234,13 +257,18 @@
 
         if step > 0:
             b = pick(z, [order[step - 1] for order in nears])
+            which = (0, 1) if step < nz - 1 else (0,)
             for d in range(1, nx):
                 block = b * nx + lax.rem(x + d, nx)
-                w_arrived(block)
+                for i in range(2):
+                    w_arrived(block, i)
                 if not whole:
-                    project(block)
+                    project(block, which=which)
             if whole:
-                project(b * nx, first=step == 1, size=nx)
+                project(b * nx, first=step == 1, size=nx, which=which)
+        if step == nz - 2:
+            for d in range(1, nx):
+                swap_copy(d).start()
 
     own_c.wait()
     lanes = 128
@@ -299,12 +327,28 @@
     fars = [far_order(at, nz) for at in range(nz)]
     order = [pick(z, [o[q] for o in fars]) for q in range(nz)]
 
-    def x_grad(b, d):
+    def hrows(i):
+        return pl.ds(i * half, half)
+
+    def x_grad(b, d, i):
         to = lax.rem(x + d, nx)
         return remote(
-            gbuf.at[b * nx + to], xrecv.at[d - 1, b], x_send.at[d - 1, b], x_recv.at[d - 1, b],
-            z * nx + to, tp,
-        )
+            gbuf.at[b * nx + to, hrows(i), :], xrecv.at[d - 1, b, hrows(i), :],
+            x_send.at[d - 1, b, i], x_recv.at[d - 1, b, i], z * nx + to, tp,
+        )
+
+    def swap_grad(d):
+        return remote(
+            gbuf.at[pair * nx + lax.rem(x + d, nx), hrows(1), :], swrecv.at[d - 1],
+            sw_send.at[d - 1], sw_recv.at[d - 1], pair * nx + x, tp,
+        )
+
+    def terms_of(b):
+        if whole:
+            weight_term(b * nx, size=nx)
+        else:
+            for d in range(1, nx):
+                weight_term(b * nx + lax.rem(x + d, nx))
 
     def tap_x(d):
         return remote(
@@ -315,12 +359,31 @@
         tap_x(d).start()
 
     for q in range(nz):
-        if whole:
-            weight_term(order[q] * nx, size=nx)
+        b = order[q]
+        if q == 0:
+            terms_of(b)
+        else:
+
+            @pl.when(b != pair)
+            def _():
+                terms_of(b)
+
         for d in range(1, nx):
-            if not whole:
-                weight_term(order[q] * nx + lax.rem(x + d, nx))
-            x_grad(order[q], d).start()
+            x_grad(b, d, 0).start()
+
+            if q < nz - 1:
+
+                @pl.when(b != pair)
+                def _():
+                    x_grad(b, d, 1).start()
+
+        if q == 0:
+            terms_of(pair)
+            for d in range(1, nx):
+                swap_grad(d).start()
+    for q in range(nz):
+        if not whole:
+            weight_term(order[q] * nx + x)
 
     def input_term(t):
         at = pl.ds(pl.multiple_of(t * part, part), part)
@@ -340,13 +403,11 @@
         to = lax.rem(tp + d, nt)
         return remote(pbuf.at[to], precv.at[d - 1], p_send.at[d - 1], p_recv.at[d - 1], me, to)
 
-    for d in range(1, nt):
-        input_term(lax.rem(tp + d, nt))
-        part_copy(d).start()
-    for q in range(nz):
-        if not whole:
-            weight_term(order[q] * nx + x)
-    input_term(tp)
+    def all_input_terms():
+        for d in range(1, nt):
+            input_term(lax.rem(tp + d, nt))
+            part_copy(d).start()
+        input_term(tp)
 
     def forward(j, carry):
         row = lax.broadcasted_iota(jnp.int32, (seq, lanes), 0)
@@ -357,7 +418,15 @@
         hidden_ref[:, at_u] = (cg * jax.nn.sigmoid(cg) * cu).astype(BF16)
         return carry
 
-    lax.fori_loop(0, cols // lanes, forward, 0)
+    def all_hidden():
+        for at in range(nz - 2, nz):
+            b = pick(z, [order[at] for order in nears])
+            if whole:
+                project(b * nx, size=nx, which=(1,))
+            else:
+                for d in range(1, nx):
+                    project(b * nx + lax.rem(x + d, nx), which=(1,))
+        lax.fori_loop(0, cols // lanes, forward, 0)
 
     total = tloc[...]
     for d in range(1, nx):
@@ -379,70 +448,91 @@
     for d in range(1, nz):
         tap_z(d).start()
 
-    def add_into(b, sources):
-        value = gbuf[b].astype(F32)
+    def add_into(b, i, sources):
+        value = gbuf[b, hrows(i), :].astype(F32)
         for source in sources:
             value = value + source[...].astype(F32)
-        gbuf[b] = value.astype(BF16)
-
-    def up_grad(b):
-        return remote(gbuf.at[b * nx + x], uprecv.at[b], up_send.at[b], up_recv.at[b], me + nx, tp)
-
-    def dn_grad(b):
-        return remote(gbuf.at[b * nx + x], dnrecv.at[b], dn_send.at[b], dn_recv.at[b], me - nx, tp)
+        gbuf[b, hrows(i), :] = value.astype(BF16)
+
+    def up_grad(b, i):
+        return remote(
+            gbuf.at[b * nx + x, hrows(i), :], uprecv.at[b, hrows(i), :],
+            up_send.at[b, i], up_recv.at[b, i], me + nx, tp,
+        )
+
+    def dn_grad(b, i):
+        return remote(
+            gbuf.at[b * nx + x, hrows(i), :], dnrecv.at[b, hrows(i), :],
+            dn_send.at[b, i], dn_recv.at[b, i], me - nx, tp,
+        )
 
     for q in range(nz):
         b = order[q]
         mine = b * nx + x
-        for d in range(1, nx):
-            x_grad(b, d).wait_recv()
-        if q < nz - 1:
-            fed = jnp.logical_or(jnp.logical_and(b > z, z > 0), jnp.logical_and(b < z, z < nz - 1))
-
-            @pl.when(jnp.logical_and(b > z, z > 0))
-            def _():
-                up_grad(b).wait_recv()
-                add_into(mine, [xrecv.at[d - 1, b] for d in range(1, nx)] + [uprecv.at[b]])
-
-            @pl.when(jnp.logical_and(b < z, z < nz - 1))
-            def _():
-                dn_grad(b).wait_recv()
-                add_into(mine, [xrecv.at[d - 1, b] for d in range(1, nx)] + [dnrecv.at[b]])
-
-            @pl.when(jnp.logical_not(fed))
-            def _():
-                add_into(mine, [xrecv.at[d - 1, b] for d in range(1, nx)])
-
-            @pl.when(b > z)
-            def _():
-                up_grad(b).start()
-
-            @pl.when(b < z)
-            def _():
-                dn_grad(b).start()
-
-        else:
-            for copy in own_s:
-                copy.wait()
-            halves = ((newup_ref, 0, pl.ds(0, cols)), (newgate_ref, 1, pl.ds(cols, cols)))
-            for new, at, lane in halves:
-                value = gbuf[mine, :, lane].astype(F32)
+        for i in range(2):
+            if q < nz - 1:
+
+                def from_x():
+                    for d in range(1, nx):
+                        x_grad(b, d, i).wait_recv()
+                    add_into(mine, i, [xrecv.at[d - 1, b, hrows(i), :] for d in range(1, nx)])
+
+                if i == 0:
+                    from_x()
+                else:
+                    pl.when(b != pair)(from_x)
+
+                @pl.when(b > z)
+                def _():
+                    @pl.when(z > 0)
+                    def _():
+                        up_grad(b, i).wait_recv()
+                        add_into(mine, i, [uprecv.at[b, hrows(i), :]])
+
+                    up_grad(b, i).start()
+
+                @pl.when(b < z)
+                def _():
+                    @pl.when(z < nz - 1)
+                    def _():
+                        dn_grad(b, i).wait_recv()
+                        add_into(mine, i, [dnrecv.at[b, hrows(i), :]])
+
+                    dn_grad(b, i).start()
+
+                continue
+            if i == 0:
+                for copy in own_s:
+                    copy.wait()
+            sides = ((newup_ref, 0, pl.ds(0, cols)), (newgate_ref, 1, pl.ds(cols, cols)))
+            for d in range(1, nx):
+                x_grad(b, d, i).wait_recv()
+            for new, at, lane in sides:
+                value = gbuf[mine, hrows(i), lane].astype(F32)
                 for d in range(1, nx):
-                    value = value + xrecv[d - 1, b, :, lane].astype(F32)
-                new[...] = oldsum[at] + scale * value
+                    value = value + xrecv[d - 1, b, hrows(i), lane].astype(F32)
+                new[hrows(i), :] = oldsum[at, hrows(i), :] + scale * value
 
             @pl.when(z > 0)
             def _():
-                up_grad(b).wait_recv()
-                for new, at, lane in halves:
-                    new[...] += scale * uprecv[b, :, lane].astype(F32)
+                up_grad(b, i).wait_recv()
+                for new, at, lane in sides:
+                    new[hrows(i), :] += scale * uprecv[b, hrows(i), lane].astype(F32)
 
             @pl.when(z < nz - 1)
             def _():
-                dn_grad(b).wait_recv()
-                for new, at, lane in halves:
-                    new[...] += scale * dnrecv[b, :, lane].astype(F32)
-
+                dn_grad(b, i).wait_recv()
+                for new, at, lane in sides:
+                    new[hrows(i), :] += scale * dnrecv[b, hrows(i), lane].astype(F32)
+
+        if q == 0:
+            for d in range(1, nx):
+                swap_grad(d).wait_recv()
+                add_into(z * nx + lax.rem(x + d, nx), 1, [swrecv.at[d - 1]])
+                x_grad(z, d, 1).start()
+            all_input_terms()
+        if q == 1:
+            all_hidden()
         if q == 0:
             total = tzrecv[nz - 1]
             for d in range(1, nz):
@@ -475,27 +565,38 @@
         tap_z(d).wait_send()
     for copy in first_rows + forwards:
         copy.wait_send()
+    for d in range(1, nx):
+        swap_copy(d).wait_send()
+        swap_grad(d).wait_send()
     for b in range(nz):
-        for copy in x_copies(b):
-            copy.wait_send()
-        for d in range(1, nx):
-            x_grad(b, d).wait_send()
-
-        @pl.when(jnp.logical_and(z < nz - 1, b <= z))
-        def _():
-            up_copy(b).wait_send()
-
-        @pl.when(jnp.logical_and(z > 0, b >= z))
-        def _():
-            dn_copy(b).wait_send()
-
-        @pl.when(b > z)
-        def _():
-            up_grad(b).wait_send()
-
-        @pl.when(b < z)
-        def _():
-            dn_grad(b).wait_send()
+        for i in range(2):
+
+            def x_left():
+                for copy in x_copies(b, i):
+                    copy.wait_send()
+                for d in range(1, nx):
+                    x_grad(b, d, i).wait_send()
+
+            if i == 0:
+                x_left()
+            else:
+                pl.when(b != pair)(x_left)
+
+            @pl.when(jnp.logical_and(z < nz - 1, b <= z))
+            def _():
+                up_copy(b, i).wait_send()
+
+            @pl.when(jnp.logical_and(z > 0, b >= z))
+            def _():
+                dn_copy(b, i).wait_send()
+
+            @pl.when(b > z)
+            def _():
+                up_grad(b, i).wait_send()
+
+            @pl.when(b < z)
+            def _():
+                dn_grad(b, i).wait_send()
 
 
 def shards(
@@ -538,6 +639,7 @@
             pltpu.VMEM((nx - 1, nz, depth, both), BF16),
             pltpu.VMEM((nz, depth, both), BF16),
             pltpu.VMEM((nz, depth, both), BF16),
+            pltpu.VMEM((nx - 1, depth // 2, both), BF16),
             pltpu.VMEM((nt, part, width), BF16),
             pltpu.VMEM((nt - 1, part, width), BF16),
             pltpu.VMEM((2, depth, cols), F32),
@@ -547,19 +649,22 @@
             pltpu.VMEM((nz, 8, cols), F32),
             pltpu.VMEM((nt, 8, cols), F32),
             dma((7,)),
-            dma((nf,)),
-            dma((nz,)),
-            dma((nz,)),
-            dma((nx - 1, nz)),
+            dma((nf, 2)),
+            dma((nz, 2)),
+            dma((nz, 2)),
+            dma((nx - 1, nz, 2)),
+            dma((nx - 1,)),
             dma((2, nt)),
             dma((2, nt)),
             dma((2, nt)),
-            dma((nx - 1, nz)),
-            dma((nx - 1, nz)),
-            dma((nz,)),
-            dma((nz,)),
-            dma((nz,)),
-            dma((nz,)),
+            dma((nx - 1, nz, 2)),
+            dma((nx - 1, nz, 2)),
+            dma((nx - 1,)),
+            dma((nx - 1,)),
+            dma((nz, 2)),
+            dma((nz, 2)),
+            dma((nz, 2)),
+            dma((nz, 2)),
             dma((nt - 1,)),
             dma((nt - 1,)),
             dma((nx - 1,)),

time: 171 us -> 165 us (0.965)
  the two profiles are of different devices: /device:TPU:8 before, /device:TPU:24 now
where the time goes in v3:
time: 165 us
  Pallas kernels  157 us (95%)
  local copies, waits for them, and re-layouts  7.18 us (4%)
    pallas_call x1, Pallas kernels, shards(): pl.pallas_call(functools.partial(kernel, nx, nz, nt, scale), out_shape=(j...  157 us
    unnamed x16, local copies, waits for them, and re-layouts  7.18 us

profile of v3, /device:TPU:24, one launch (start us, length us, event | category | flops | bytes accessed | tf_op | source)
XLA Modules:
  0.0 164.6 jit_solution(540801978478138081)
XLA Ops:
  0.6 156.8 %layer.1 = (bf16[512,768]{1,0:T(8,128)(2,1)}, bf16[128,2048]{1,0:T(8,128)(2,1)}, f32[256,768]{1,0:T(8,128)}, f32[256,768]{1,0:T(8,128)}, f32[3,3072]{1,0:T(4,128)}, /*index=5*/f32[3,3072]{1,0:T(4,128)}) custom-call(bf16[128,2048]{1,0:T(8,128)(2,1)} %later_hbm.1, bf16[128,2048]{1,0:T(8,128)(2,1)} %saved_hbm.1, bf16[512,768]{1,0:T(8,128)(2,1)} %cot_hbm.1, ...), custom_call_target="tpu_custom_call" | custom-call | tf_op jit(solution)/shard_map/layer/pallas_call | solution.py:618
  157.4 0.0 copy-start.2
  157.4 2.1 %copy.23 = bf16[512,768]{1,0:T(8,128)(2,1)} copy(bf16[512,768]{1,0:T(8,128)(2,1)} %get-tuple-element.12) | data formatting | bytes 1572864
  159.5 0.0 copy-done.2
  159.5 0.0 copy-start.1
  159.5 0.8 copy.24
  160.3 0.5 copy-done.1
  160.9 0.0 copy-start
  160.9 0.9 copy.25
  161.8 0.5 copy-done
  162.3 0.0 copy-start.4
  162.3 0.9 copy.26
  163.2 0.0 copy-done.4
  163.2 0.0 copy-start.3
  163.2 0.6 copy.27
  163.8 0.2 copy-done.3
  164.0 0.6 copy.28
Async XLA Ops:
  157.4 2.1 %copy-start.2 = (bf16[128,2048]{1,0:T(8,128)(2,1)S(1)}, bf16[128,2048]{1,0:T(8,128)(2,1)}, u32[]{:S(2)}) copy-start(bf16[128,2048]{1,0:T(8,128)(2,1)} %get-tuple-element.13) | copy-start | bytes 1572868
  159.5 1.3 copy-start.1
  160.9 1.4 copy-start
  162.3 0.9 copy-start.4
  163.2 0.8 copy-start.3

commit v4 on v3

--- a/solution.py
+++ b/solution.py
@@ -206,69 +206,85 @@
 
     nears = [near_order(at, nz) for at in range(nz)]
     forwards = []
-    for step in range(nz + 1):
-        if 0 < step < nz:
+    def pass_rows(a):
+        for d in range(1, chips):
+            owner = lax.rem(chip + d, chips) * CORES + core
+            row_arrived(a, owner)
+            copy = row_copy(a, owner, mate, r_fwd.at[a, d])
+            copy.start()
+            forwards.append(copy)
+
+    def pass_z(step, i):
+        low, high = z - step, z + step
+
+        @pl.when(low >= 0)
+        def _():
+            w_arrived(low * nx + x, i)
+
+            @pl.when(z < nz - 1)
+            def _():
+                up_copy(low, i).start()
+
+            pass_x(low, i)
+
+        @pl.when(high < nz)
+        def _():
+            w_arrived(high * nx + x, i)
+
+            @pl.when(z > 0)
+            def _():
+                dn_copy(high, i).start()
+
+            pass_x(high, i)
+
+    def project_z(step):
+        if not whole:
             low, high = z - step, z + step
 
+            @pl.when(low >= 0)
+            def _():
+                project(low * nx + x)
+
+            @pl.when(high < nz)
+            def _():
+                project(high * nx + x)
+
+    def from_x(at):
+        b = pick(z, [order[at] for order in nears])
+        which = (0, 1) if at < nz - 2 else (0,)
+        for d in range(1, nx):
+            block = b * nx + lax.rem(x + d, nx)
             for i in range(2):
-
-                @pl.when(low >= 0)
-                def _():
-                    w_arrived(low * nx + x, i)
-
-                    @pl.when(z < nz - 1)
-                    def _():
-                        up_copy(low, i).start()
-
-                    pass_x(low, i)
-
-                @pl.when(high < nz)
-                def _():
-                    w_arrived(high * nx + x, i)
-
-                    @pl.when(z > 0)
-                    def _():
-                        dn_copy(high, i).start()
-
-                    pass_x(high, i)
-
-        if step == 1:
-            for a in range(2):
-                for d in range(1, chips):
-                    owner = lax.rem(chip + d, chips) * CORES + core
-                    row_arrived(a, owner)
-                    copy = row_copy(a, owner, mate, r_fwd.at[a, d])
-                    copy.start()
-                    forwards.append(copy)
+                w_arrived(block, i)
+            if not whole:
+                project(block, which=which)
+        if whole:
+            project(b * nx, first=at == 0, size=nx, which=which)
+
+    for step in range(1, nz):
+        pass_z(step, 0)
+        if step == 2:
+            pass_rows(1)
             for a in range(2):
                 for d in range(chips):
                     row_arrived(a, lax.rem(chip + d, chips) * CORES + (CORES - 1 - core))
             if not whole:
                 project(me, first=True)
-        if 0 < step < nz and not whole:
-
-            @pl.when(low >= 0)
-            def _():
-                project(low * nx + x)
-
-            @pl.when(high < nz)
-            def _():
-                project(high * nx + x)
-
-        if step > 0:
-            b = pick(z, [order[step - 1] for order in nears])
-            which = (0, 1) if step < nz - 1 else (0,)
-            for d in range(1, nx):
-                block = b * nx + lax.rem(x + d, nx)
-                for i in range(2):
-                    w_arrived(block, i)
-                if not whole:
-                    project(block, which=which)
-            if whole:
-                project(b * nx, first=step == 1, size=nx, which=which)
-        if step == nz - 2:
-            for d in range(1, nx):
-                swap_copy(d).start()
+            project_z(1)
+        if step > 2:
+            from_x(step - 2)
+        pass_z(step, 1)
+        if step == 1:
+            pass_rows(0)
+        else:
+            if step == 2:
+                from_x(0)
+            if step == nz - 2:
+                for d in range(1, nx):
+                    swap_copy(d).start()
+            project_z(step)
+    for at in range(nz - 2, nz):
+        from_x(at)
 
     own_c.wait()
     lanes = 128

time: 165 us -> 151 us (0.915)
  Pallas kernels: 157 us -> 143 us
    pallas_call x1, Pallas kernels: 157 us -> 143 us  [shards(): pl.pallas_call(functools.partial(kernel, nx, nz, nt, scale), out_shape=(j...]
where the time goes in v4:
time: 151 us
  Pallas kernels  143 us (95%)
  local copies, waits for them, and re-layouts  7.18 us (5%)
    pallas_call x1, Pallas kernels, shards(): pl.pallas_call(functools.partial(kernel, nx, nz, nt, scale), out_shape=(j...  143 us
    unnamed x16, local copies, waits for them, and re-layouts  7.18 us

profile of v4, /device:TPU:24, one launch (start us, length us, event | category | flops | bytes accessed | tf_op | source)
XLA Modules:
  0.0 150.6 jit_solution(7678810243499357706)
XLA Ops:
  0.6 142.8 %layer.1 = (bf16[512,768]{1,0:T(8,128)(2,1)}, bf16[128,2048]{1,0:T(8,128)(2,1)}, f32[256,768]{1,0:T(8,128)}, f32[256,768]{1,0:T(8,128)}, f32[3,3072]{1,0:T(4,128)}, /*index=5*/f32[3,3072]{1,0:T(4,128)}) custom-call(bf16[128,2048]{1,0:T(8,128)(2,1)} %later_hbm.1, bf16[128,2048]{1,0:T(8,128)(2,1)} %saved_hbm.1, bf16[512,768]{1,0:T(8,128)(2,1)} %cot_hbm.1, ...), custom_call_target="tpu_custom_call" | custom-call | tf_op jit(solution)/shard_map/layer/pallas_call | solution.py:634
  143.4 0.0 copy-start.2
  143.5 2.1 %copy.23 = bf16[512,768]{1,0:T(8,128)(2,1)} copy(bf16[512,768]{1,0:T(8,128)(2,1)} %get-tuple-element.12) | data formatting | bytes 1572864
  145.6 0.0 copy-done.2
  145.6 0.0 copy-start.1
  145.6 0.8 copy.24
  146.4 0.5 copy-done.1
  146.9 0.0 copy-start
  146.9 0.9 copy.25
  147.8 0.5 copy-done
  148.3 0.0 copy-start.4
  148.3 0.9 copy.26
  149.2 0.0 copy-done.4
  149.2 0.0 copy-start.3
  149.2 0.6 copy.27
  149.8 0.2 copy-done.3
  150.0 0.6 copy.28
Async XLA Ops:
  143.4 2.1 %copy-start.2 = (bf16[128,2048]{1,0:T(8,128)(2,1)S(1)}, bf16[128,2048]{1,0:T(8,128)(2,1)}, u32[]{:S(2)}) copy-start(bf16[128,2048]{1,0:T(8,128)(2,1)} %get-tuple-element.13) | copy-start | bytes 1572868
  145.6 1.3 copy-start.1
  146.9 1.4 copy-start
  148.3 0.9 copy-start.4
  149.2 0.8 copy-start.3
